TPU v7x, 32 devices: a whole 2x2x4 slice. The times are simulated.
32 devices in a mesh: grp: 2 (over y), sp: 4 (over z), tp: 4 (over x, core).
Axes of the slice: x: 2, y: 2, z: 4, core: 2. Of those that a mesh axis runs over, the one named last changes fastest.
Arguments:
- tokens: bfloat16 [4096, 2048], P(('grp', 'sp', 'tp')), parts along dimension 0, may hold values from -6 to 6
- norm_gain: bfloat16 [2048], replicated, may hold values from 0.099609375 to 1.8984375
- conv_outer_weight: bfloat16 [2048, 1024], P('sp', 'tp'), may hold values from -0.125 to 0.125
- conv_inner_weight: bfloat16 [2048, 1024], P('sp', 'tp'), may hold values from -0.125 to 0.125
- conv_input_weight: bfloat16 [2048, 1024], P('sp', 'tp'), may hold values from -0.125 to 0.125
- query_matrix: bfloat16 [2048, 1024], P('sp', 'tp'), may hold values from -0.125 to 0.125
- key_weight: bfloat16 [2048, 1024], P('sp', 'tp'), may hold values from -0.125 to 0.125
- value_weight: bfloat16 [2048, 1024], P('sp', 'tp'), may hold values from -0.125 to 0.125
- gate_weight: bfloat16 [2048, 1024], P('sp', 'tp'), may hold values from -0.125 to 0.125
- conv_taps: bfloat16 [3, 1024], P(None, 'tp'), may hold values from -3.5 to 3.5
- conv_out_weight: bfloat16 [1024, 2048], P('tp', 'sp'), may hold values from -0.125 to 0.125
- ret_out_weight: bfloat16 [1024, 2048], P('tp', 'sp'), may hold values from -0.125 to 0.125
- log_decay: float32 [4096, 8], P(('grp', 'sp'), 'tp'), parts along dimension 0, may hold values from -0.75 to 0
Outputs:
- mixed: bfloat16 [4096, 2048], P(('grp', 'sp', 'tp')), parts along dimension 0
There are 2 independent parts, one for each index of `grp`. A program takes and returns all parts, laid end to end along the dimension named above; an argument that names none is the same for every part. Nothing has to cross between parts.
All inputs are finite; a program needn't handle non-finite values.
Results may differ from a plain program's by a relative error of at most 0.025.
Values may be sent and summed in bfloat16 or wider, within the bound.
A program may use at most 64 MiB of HBM per device.

v0:
```python
import jax
import jax.numpy as jnp
from jax import lax
from jax.sharding import PartitionSpec as P

HEAD = 128
CONV_K = 3
BLOCK = 128
EPSILON = 1e-06
ROTARY_BASE = 10000.0
HIGHEST_PRECISION = lax.Precision.HIGHEST


def prefix_2(x, axis, join, neutral):
    place = lax.axis_index(axis)
    gathered = jax.tree.map(
        lambda a, kind: lax.all_gather(a.astype(kind), axis), x, (jnp.bfloat16, jnp.bfloat16)
    )
    state = jax.tree.map(lambda a, e: jnp.zeros_like(a) + jnp.asarray(e, a.dtype), x, neutral)

    def one(turn, state):
        return join(
            state,
            jax.tree.map(
                lambda a, own: lax.dynamic_index_in_dim(a, turn, 0, False).astype(own.dtype),
                gathered,
                x,
            ),
        )

    return lax.fori_loop(0, place, one, state)


def shifted(x, axis, by):
    count = lax.axis_size(axis)
    pairs = [(i, i + by) for i in range(count) if 0 <= i + by < count]
    return lax.ppermute(x, axis, pairs)


def rotate(head_data, positions):
    half_width = head_data.shape[-1] // 2
    inv_freq = ROTARY_BASE ** (-jnp.arange(half_width, dtype=jnp.float32) / half_width)
    angles = positions[:, None] * inv_freq[None, :]
    cosine = jnp.cos(angles)[:, None, :]
    sine_part = jnp.sin(angles)[:, None, :]
    first_half = head_data[..., :half_width]
    second_half = head_data[..., half_width:]
    return jnp.concatenate(
        [
            first_half * cosine - second_half * sine_part,
            second_half * cosine + first_half * sine_part,
        ],
        axis=-1,
    )


def head_norm(head_data):
    return head_data * lax.rsqrt(jnp.mean(head_data * head_data, axis=-1, keepdims=True) + EPSILON)


def combine_states(earlier, later):
    return (earlier[0] * later[0], later[0][:, None, None] * earlier[1] + later[1])


def body(
    tokens,
    norm_gain,
    conv_outer_weight,
    conv_inner_weight,
    conv_input_weight,
    query_matrix,
    key_weight,
    value_weight,
    gate_weight,
    conv_taps,
    conv_out_weight,
    ret_out_weight,
    log_decay,
):
    values32 = tokens.astype(jnp.float32)
    normed = (
        values32
        * lax.rsqrt(jnp.mean(values32 * values32, axis=-1, keepdims=True) + EPSILON)
        * norm_gain.astype(jnp.float32)
    ).astype(jnp.bfloat16)
    gathered = lax.all_gather(normed, "tp", axis=0, tiled=True)
    row_total = gathered.shape[0]
    whole = (
        lax.all_gather(conv_outer_weight, "sp", axis=0, tiled=True),
        lax.all_gather(conv_inner_weight, "sp", axis=0, tiled=True),
        lax.all_gather(conv_input_weight, "sp", axis=0, tiled=True),
        lax.all_gather(query_matrix, "sp", axis=0, tiled=True),
        lax.all_gather(key_weight, "sp", axis=0, tiled=True),
        lax.all_gather(value_weight, "sp", axis=0, tiled=True),
        lax.all_gather(gate_weight, "sp", axis=0, tiled=True),
    )
    projected = tuple(
        (
            jnp.dot(gathered, weight, preferred_element_type=jnp.float32).astype(jnp.bfloat16)
            for weight in whole
        )
    )
    conv_outer, conv_inner, conv_input, query_proj, key_proj, value_proj, gate_proj = projected
    heads_here = query_proj.shape[1] // HEAD
    offset = (lax.axis_index("sp") * row_total).astype(jnp.float32)
    positions = offset + jnp.arange(row_total, dtype=jnp.float32)
    head_shape = (row_total, heads_here, HEAD)
    queries = rotate(query_proj.astype(jnp.float32).reshape(head_shape), positions)
    keys_rot = rotate(key_proj.astype(jnp.float32).reshape(head_shape), positions) * HEAD ** (-0.5)
    head_values = value_proj.astype(jnp.float32).reshape(head_shape)
    block_count = row_total // BLOCK
    block_shape = (block_count, BLOCK, heads_here, HEAD)
    query_blocks = queries.reshape(block_shape)
    key_blocks = keys_rot.reshape(block_shape)
    value_blocks = head_values.reshape(block_shape)
    log_blocks = log_decay.reshape(block_count, BLOCK, heads_here)
    offsets = jnp.arange(BLOCK, dtype=jnp.int32)
    causal_mask = offsets[:, None] >= offsets[None, :]
    lower_ones = causal_mask.astype(jnp.float32)
    cumulative = jnp.einsum("ij,njh->nih", lower_ones, log_blocks, precision=HIGHEST_PRECISION)
    block_end = cumulative[:, -1, :]
    mixed_in = conv_inner.astype(jnp.float32) * conv_input.astype(jnp.float32)
    rim = shifted(mixed_in[row_total - (CONV_K - 1) :], "sp", 1)
    extended = jnp.concatenate([rim, mixed_in], axis=0)
    taps = conv_taps.astype(jnp.float32)
    conv_out = jnp.zeros(mixed_in.shape, jnp.float32)
    for tap_index in range(CONV_K):
        conv_out = conv_out + taps[tap_index][None, :] * extended[tap_index : tap_index + row_total]
    conv_branch = (conv_outer.astype(jnp.float32) * conv_out).astype(jnp.bfloat16)
    weights = jnp.exp(block_end[:, None, :] - cumulative)
    increments = jnp.einsum(
        "njh,njhd,njhe->nhde", weights, key_blocks, value_blocks, precision=HIGHEST_PRECISION
    )

    def carry_on(carried, pieces):
        block_decay, increment = pieces
        return (block_decay[:, None, None] * carried + increment, carried)

    start_state = jnp.zeros((heads_here, HEAD, HEAD), jnp.float32)
    local_end, local_before = lax.scan(carry_on, start_state, (jnp.exp(block_end), increments))
    device_decay = jnp.exp(jnp.sum(block_end, axis=0))
    incoming = prefix_2(
        (device_decay, local_end),
        "sp",
        combine_states,
        (jnp.ones_like(device_decay), jnp.zeros_like(local_end)),
    )
    local_before, incoming_state = (local_before, incoming[1])
    spread = cumulative[:, :, None, :] - cumulative[:, None, :, :]
    grid_mask = causal_mask[None, :, :, None]
    decay_grid = jnp.where(grid_mask, jnp.exp(jnp.where(grid_mask, spread, 0.0)), 0.0)
    scores = (
        jnp.einsum("nihd,njhd->nijh", query_blocks, key_blocks, precision=HIGHEST_PRECISION)
        * decay_grid
    )
    within = jnp.einsum("nijh,njhe->nihe", scores, value_blocks, precision=HIGHEST_PRECISION)
    prefix = jnp.exp(jnp.cumsum(block_end, axis=0) - block_end)
    before = local_before + prefix[:, :, None, None] * incoming_state[None]
    across = jnp.einsum("nihd,nhde->nihe", query_blocks, before, precision=HIGHEST_PRECISION)
    across = across * jnp.exp(cumulative)[..., None]
    retained = (within + across).reshape(head_shape)
    ret_branch = (
        head_norm(retained).reshape(row_total, heads_here * HEAD)
        * jax.nn.silu(gate_proj.astype(jnp.float32))
    ).astype(jnp.bfloat16)
    conv_rows_weight, ret_rows_weight = (
        lax.all_gather(conv_out_weight, "sp", axis=1, tiled=True),
        lax.all_gather(ret_out_weight, "sp", axis=1, tiled=True),
    )
    return lax.psum_scatter(
        (
            jnp.dot(conv_branch, conv_rows_weight, preferred_element_type=jnp.float32)
            + jnp.dot(ret_branch, ret_rows_weight, preferred_element_type=jnp.float32)
        ).astype(jnp.bfloat16),
        "tp",
        scatter_dimension=0,
        tiled=True,
    )


def solution(mesh):
    placed = (
        P(("grp", "sp", "tp"), None),
        P(),
        P("sp", "tp"),
        P("sp", "tp"),
        P("sp", "tp"),
        P("sp", "tp"),
        P("sp", "tp"),
        P("sp", "tp"),
        P("sp", "tp"),
        P(None, "tp"),
        P("tp", "sp"),
        P("tp", "sp"),
        P(("grp", "sp"), "tp"),
    )
    return jax.shard_map(
        body, mesh=mesh, in_specs=placed, out_specs=P(("grp", "sp", "tp"), None), check_vma=False
    )
```

profile of v0, /device:TPU:0, one launch (start us, length us, event | category | flops | bytes accessed | tf_op | source)
XLA Modules:
  0.0 343.9 jit_solution(5092971589011308150)
XLA Ops:
  6.5 0.7 all-gather.25.cloned.1.call-update
  7.3 0.7 convert_element_type.96
  8.0 1.3 fusion.9
  9.3 2.0 fusion.11
  11.4 0.7 all-gather.27.cloned.1.call-update
  13.9 0.7 all-gather.15.cloned.1.call-update
  14.6 0.7 all-gather.21.cloned.1.call-update
  15.4 0.7 all-gather.29.cloned.1.call-update
  20.9 14.0 %all-reduce = bf16[8]{0:T(256)(128)(2,1)S(1)} all-reduce(bf16[8]{0:T(256)(128)(2,1)S(1)} %dynamic-update-slice), channel_id=2, replica_groups=mesh['grp'=2,'sp'=4,'tp'=4] {'sp'}, use_global_device_ids=true, to_apply=%add | all-reduce | flops 8 | bytes 32
  37.4 1.8 multiply_cosine_fusion
  39.2 0.7 all-gather.25.cloned.1.call-done
  39.9 23.6 %all-gather.13.cloned.1.call-done = bf16[512,2048]{1,0:T(8,128)(2,1)} async-done(((bf16[128,2048]{1,0:T(8,128)(2,1)}), bf16[512,2048]{1,0:T(8,128)(2,1)}) %all-gather.13.cloned.1.call-update) | async-done | bytes 2097168 | tf_op jit(solution)/shard_map/all_gather | solution.py:86
  63.5 2.6 convolution_convert_fusion.2
  66.2 1.0 copy.95
  67.2 1.0 copy.96
  68.2 24.9 %all-gather.27.cloned.1.call-done = bf16[2048,256]{1,0:T(8,128)(2,1)} async-done(((bf16[512,256]{1,0:T(8,128)(2,1)}), bf16[2048,256]{1,0:T(8,128)(2,1)}) %all-gather.27.cloned.1.call-update) | async-done | bytes 1048592 | tf_op jit(solution)/shard_map/all_gather | solution.py:92
  93.1 2.0 convolution_convert_fusion.1
  95.1 1.0 copy.97
  96.1 1.0 copy.98
  97.1 24.8 %all-gather.23.cloned.1.call-done = bf16[2048,256]{1,0:T(8,128)(2,1)} async-done(((bf16[512,256]{1,0:T(8,128)(2,1)}), bf16[2048,256]{1,0:T(8,128)(2,1)}) %all-gather.23.cloned.1.call-update) | async-done | bytes 1048592 | tf_op jit(solution)/shard_map/all_gather | solution.py:94
  121.9 1.9 convolution_convert_fusion.3
  123.9 2.9 multiply_subtract_fusion
  126.8 1.7 fusion.23
  128.5 9.4 %while.26 = (s32[]{:T(128)}, f32[2,128,128]{2,1,0:T(8,128)S(1)}, f32[4,2,128,128]{3,2,1,0:T(8,128)}, f32[4,2]{1,0:T(4,128)}, f32[4,2,128,128]{3,2,1,0:T(8,128)}, /*index=5*/s32[]{:T(128)}, s32[]{:T(128)}) while((s32[]{:T(128)}, f32[2,128,128]{2,1,0:T(8,128)S(1)}, f32[4,2,128,128]{3,2,1,0:T(8,128)}, f32[4,2]{1,0:T(4,128)}, ...), condition=%wide.region_2.3_spmd.clone, body=%wide.region_1.2_spmd.clone.sunk | while | flops 131075 | bytes 655992 | solution.py:140
  129.1 0.7 fusion.69
  129.8 1.0 bitcast_add_fusion.2
  131.5 0.7 fusion.69
  132.1 1.0 bitcast_add_fusion.2
  133.1 0.7 bitcast_dynamic-update-slice_fusion.2
  133.8 0.7 fusion.69
  134.5 1.0 bitcast_add_fusion.2
  135.5 0.7 bitcast_dynamic-update-slice_fusion.2
  136.8 1.0 bitcast_add_fusion.2
  137.9 17.1 %all-gather.1 = bf16[8,128,128]{2,1,0:T(8,128)(2,1)} all-gather(bf16[2,128,128]{2,1,0:T(8,128)(2,1)S(1)} %convert_element_type.112), channel_id=3, replica_groups=mesh['grp'=2,'sp'=4,'tp'=4] {'sp'}, dimensions={0}, use_global_device_ids=true | all-gather | bytes 327680 | tf_op jit(solution)/shard_map/all_gather | solution.py:17
  155.0 2.7 fusion.7
  157.7 26.0 %all-gather.17.cloned.1.call-done = bf16[2048,256]{1,0:T(8,128)(2,1)} async-done(((bf16[512,256]{1,0:T(8,128)(2,1)}), bf16[2048,256]{1,0:T(8,128)(2,1)}) %all-gather.17.cloned.1.call-update) | async-done | bytes 1048592 | tf_op jit(solution)/shard_map/all_gather | solution.py:90
  183.7 2.2 fusion.6
  186.6 3.9 %collective-permute-start = (f32[2,256]{1,0:T(2,128)}, f32[2,256]{1,0:T(2,128)}, u32[]{:S(2)}, u32[]{:S(2)}) collective-permute-start(f32[2,256]{1,0:T(2,128)} %slice.45), channel_id=1, source_target_pairs={{0,4},{4,8},{8,12},{1,5},{5,9},{9,13},{2,6},{6,10},{10,14},{3,7},{... | collective-permute-start | bytes 6152 | tf_op jit(solution)/shard_map/ppermute | solution.py:37
  190.7 1.3 fusion.3
  192.5 1.9 multiply_reduce_fusion
  194.5 1.3 copy.85
  195.8 16.9 %all-gather.15.cloned.1.call-done = bf16[2048,256]{1,0:T(8,128)(2,1)} async-done(((bf16[512,256]{1,0:T(8,128)(2,1)}), bf16[2048,256]{1,0:T(8,128)(2,1)}) %all-gather.15.cloned.1.call-update) | async-done | bytes 1048592 | tf_op jit(solution)/shard_map/all_gather | solution.py:89
  212.7 29.0 %all-gather.21.cloned.1.call-done = bf16[256,2048]{1,0:T(8,128)(2,1)} async-done(((bf16[256,512]{1,0:T(8,128)(2,1)}), bf16[256,2048]{1,0:T(8,128)(2,1)}) %all-gather.21.cloned.1.call-update) | async-done | bytes 1048592 | tf_op jit(solution)/shard_map/all_gather | solution.py:167
  241.7 5.8 %fusion.30 = f32[512,2048]{1,0:T(8,128)} fusion(bf16[256,2048]{1,0:T(8,128)(2,1)} %all-gather.21.cloned.1.call-done, f32[2,256]{1,0:T(2,128)} %collective-permute-done, f32[512,256]{1,0:T(8,128)S(1)} %copy-done.2, bf16[512,2048]{1,0:T(8,128)(2,1)S(1)} %copy-done, bf16[2048,256]{1,0:T(8,128)(2,1)} %all-gather.15.cloned.1.call-done, f32[256]{0:T(256)S(1)} %bitcast.101, ...), kind=kOutput, calls=%fused_computation.62 | convolution fusion | flops 1075183616 | bytes 8918016 | tf_op jit(solution)/shard_map/dot_general | solution.py:172
  247.5 23.1 %all-gather.29.cloned.1.call-done = bf16[2048,256]{1,0:T(8,128)(2,1)} async-done(((bf16[512,256]{1,0:T(8,128)(2,1)}), bf16[2048,256]{1,0:T(8,128)(2,1)}) %all-gather.29.cloned.1.call-update) | async-done | bytes 1048592 | tf_op jit(solution)/shard_map/all_gather | solution.py:95
  270.6 28.8 %all-gather.31.cloned.1.call-done = bf16[256,2048]{1,0:T(8,128)(2,1)} async-done(((bf16[256,512]{1,0:T(8,128)(2,1)}), bf16[256,2048]{1,0:T(8,128)(2,1)}) %all-gather.31.cloned.1.call-update) | async-done | bytes 1048592 | tf_op jit(solution)/shard_map/all_gather | solution.py:168
  300.0 6.5 %add_convert_fusion = bf16[512,2048]{1,0:T(8,128)(2,1)} fusion(f32[512,2048]{1,0:T(8,128)} %fusion.30, bf16[256,2048]{1,0:T(8,128)(2,1)} %all-gather.31.cloned.1.call-done, f32[64,8,2,128]{3,2,1,0:T(2,128)S(1)} %bitcast.95, f32[64,8,2,128]{3,2,1,0:T(2,128)S(1)} %bitcast.94, bf16[512,2048]{1,0:T(8,128)(2,1)S(1)} %copy-done, ...), kind=kOutput, calls=%fused_computation.6 | convolution fusion | flops 1077018624 | bytes 11534336 | tf_op jit(solution)/shard_map/dot_general | solution.py:173
  306.6 30.7 %reduce-scatter.2.cloned.1.call-done = bf16[128,2048]{1,0:T(8,128)(2,1)} async-done(((bf16[512,2048]{1,0:T(8,128)(2,1)}), bf16[128,2048]{1,0:T(8,128)(2,1)}) %reduce-scatter.2.cloned.1.call-update) | async-done | bytes 524304 | tf_op jit(solution)/shard_map/reduce_scatter | solution.py:170
  (90 shorter events, 12.9 us)
Async XLA Ops:
  6.5 33.4 %all-gather.25.cloned.1.call-start = ((), (), s32[]{:S(2)}) async-start(), calls=%async_computation.7 | async-start | bytes 1310720 | tf_op jit(solution)/shard_map/all_gather | solution.py:93
  7.3 56.2 %all-gather.13.cloned.1.call-start = ((), (), s32[]{:S(2)}) async-start(), calls=%async_computation.1 | async-start | bytes 2621440 | tf_op jit(solution)/shard_map/all_gather | solution.py:86
  8.0 8.7 %copy-start.14 = (f32[512,2]{0,1:T(2,128)S(1)}, f32[512,2]{0,1:T(2,128)}, u32[]{:S(2)}) copy-start(f32[512,2]{0,1:T(2,128)} %param.29) | copy-start | bytes 12292
  8.0 10.7 %copy-start.15 = (u32[32]{0:T(128)S(1)}, u32[32]{0:T(128)}, u32[]{:S(2)}) copy-start(u32[32]{0:T(128)} %constant.65) | copy-start | bytes 388
  8.0 28.8 %copy-start.10 = (bf16[3,256]{1,0:T(4,128)(2,1)S(1)}, bf16[3,256]{1,0:T(4,128)(2,1)}, u32[]{:S(2)}) copy-start(bf16[3,256]{1,0:T(4,128)(2,1)} %param.26) | copy-start | bytes 4612
  11.3 81.8 %all-gather.27.cloned.1.call-start = ((), (), s32[]{:S(2)}) async-start(), calls=%async_computation.8 | async-start | bytes 1310720 | tf_op jit(solution)/shard_map/all_gather | solution.py:92
  12.1 109.8 %all-gather.23.cloned.1.call-start = ((), (), s32[]{:S(2)}) async-start(), calls=%async_computation.6 | async-start | bytes 1310720 | tf_op jit(solution)/shard_map/all_gather | solution.py:94
  12.6 142.4 %all-gather.19.cloned.1.call-start = ((), (), s32[]{:S(2)}) async-start(), calls=%async_computation.4 | async-start | bytes 1310720 | tf_op jit(solution)/shard_map/all_gather | solution.py:91
  13.2 170.5 %all-gather.17.cloned.1.call-start = ((), (), s32[]{:S(2)}) async-start(), calls=%async_computation.3 | async-start | bytes 1310720 | tf_op jit(solution)/shard_map/all_gather | solution.py:90
  13.8 198.9 %all-gather.15.cloned.1.call-start = ((), (), s32[]{:S(2)}) async-start(), calls=%async_computation.2 | async-start | bytes 1310720 | tf_op jit(solution)/shard_map/all_gather | solution.py:89
  14.6 227.1 %all-gather.21.cloned.1.call-start = ((), (), s32[]{:S(2)}) async-start(), calls=%async_computation.5 | async-start | bytes 1310720 | tf_op jit(solution)/shard_map/all_gather | solution.py:167
  15.3 255.3 %all-gather.29.cloned.1.call-start = ((), (), s32[]{:S(2)}) async-start(), calls=%async_computation.9 | async-start | bytes 1310720 | tf_op jit(solution)/shard_map/all_gather | solution.py:95
  16.0 283.4 %all-gather.31.cloned.1.call-start = ((), (), s32[]{:S(2)}) async-start(), calls=%async_computation.10 | async-start | bytes 1310720 | tf_op jit(solution)/shard_map/all_gather | solution.py:168
  16.6 320.7 %reduce-scatter.2.cloned.1.call-start = ((), (), s32[]{:S(2)}) async-start(), calls=%async_computation.11 | async-start | bytes 2621440 | tf_op jit(solution)/shard_map/reduce_scatter | solution.py:170
  66.1 27.0 %copy-start = (bf16[512,2048]{1,0:T(8,128)(2,1)S(1)}, bf16[512,2048]{1,0:T(8,128)(2,1)}, u32[]{:S(2)}) copy-start(bf16[512,2048]{1,0:T(8,128)(2,1)} %all-gather.13.cloned.1.call-done) | copy-start | bytes 6291460
  123.9 2.9 copy-start.8
  183.7 6.7 %copy-start.3 = (f32[512,2,64]{2,0,1:T(8,128)S(1)}, f32[512,2,64]{2,0,1:T(8,128)}, u32[]{:S(2)}) copy-start(f32[512,2,64]{2,0,1:T(8,128)} %get-tuple-element.140) | copy-start | bytes 786436
  183.7 6.7 %copy-start.4 = (f32[512,2,64]{2,0,1:T(8,128)S(1)}, f32[512,2,64]{2,0,1:T(8,128)}, u32[]{:S(2)}) copy-start(f32[512,2,64]{2,0,1:T(8,128)} %get-tuple-element.141) | copy-start | bytes 786436
  183.7 6.9 %copy-start.6 = (f32[4,128,2]{1,2,0:T(2,128)S(1)}, f32[4,128,2]{1,2,0:T(2,128)}, u32[]{:S(2)}) copy-start(f32[4,128,2]{1,2,0:T(2,128)} %copy.73) | copy-start | bytes 12292
  185.9 4.5 %copy-start.1 = (f32[512,256]{1,0:T(8,128)}, f32[512,256]{1,0:T(8,128)S(1)}, u32[]{:S(2)}) copy-start(f32[512,256]{1,0:T(8,128)S(1)} %fusion.6) | copy-start | bytes 1572868
  186.6 55.1 %collective-permute-start = (f32[2,256]{1,0:T(2,128)}, f32[2,256]{1,0:T(2,128)}, u32[]{:S(2)}, u32[]{:S(2)}) collective-permute-start(f32[2,256]{1,0:T(2,128)} %slice.45), channel_id=1, source_target_pairs={{0,4},{4,8},{8,12},{1,5},{5,9},{9,13},{2,6},{6,10},{10,14},{3,7},{... | collective-permute-start | bytes 6152 | tf_op jit(solution)/shard_map/ppermute | solution.py:37
  190.6 1.8 copy-start.5
  190.7 1.8 copy-start.7
  190.7 1.8 copy-start.9
  192.4 49.2 %copy-start.2 = (f32[512,256]{1,0:T(8,128)S(1)}, f32[512,256]{1,0:T(8,128)}, u32[]{:S(2)}) copy-start(f32[512,256]{1,0:T(8,128)} %copy-done.1) | copy-start | bytes 1572868
  192.4 49.2 %copy-start.11 = (f32[1,256]{1,0:T(1,128)S(1)}, f32[1,256]{1,0:T(1,128)}, u32[]{:S(2)}) copy-start(f32[1,256]{1,0:T(1,128)} %get-tuple-element.154) | copy-start | bytes 3076
  192.4 49.2 %copy-start.12 = (f32[1,256]{1,0:T(1,128)S(1)}, f32[1,256]{1,0:T(1,128)}, u32[]{:S(2)}) copy-start(f32[1,256]{1,0:T(1,128)} %get-tuple-element.155) | copy-start | bytes 3076
  192.4 49.2 %copy-start.13 = (f32[1,256]{1,0:T(1,128)S(1)}, f32[1,256]{1,0:T(1,128)}, u32[]{:S(2)}) copy-start(f32[1,256]{1,0:T(1,128)} %get-tuple-element.156) | copy-start | bytes 3076
Sparse Core Ops, SparseCore 0:
  8.9 30.9 all-gather.24
  41.5 21.9 all-gather.12
  65.1 27.9 all-gather.26
  94.5 27.3 all-gather.22
  123.3 31.5 all-gather.18
  156.4 27.3 all-gather.16
  185.3 27.3 all-gather.14
  214.3 27.3 all-gather.20
  243.2 27.3 all-gather.28
  272.0 27.3 all-gather.30
  306.7 30.5 reduce-scatter.1
where the time goes:
time: 345 us; the launch traced here: 344 us
  waiting for transfers between devices  234 us (68%)
  blocking collectives  31.1 us (9%)
  matrix products  29.2 us (8%)
  other arithmetic  16 us (5%)
  local copies, waits for them, and re-layouts  15 us (4%)
  between operations  14.2 us (4%)
  starting transfers between devices  4.26 us (1%)
    reduce_scatter x1, waiting for transfers between devices, body(): lax.psum_scatter((jnp.dot(conv_branch, conv_rows_weight, preferred_elemen...  30.7 us
    all_gather x1, waiting for transfers between devices, body(): lax.all_gather(conv_out_weight, 'sp', axis=1, tiled=True)  29 us
    all_gather x1, waiting for transfers between devices, body(): lax.all_gather(ret_out_weight, 'sp', axis=1, tiled=True)  28.8 us
    all_gather x1, waiting for transfers between devices, body(): lax.all_gather(conv_inner_weight, 'sp', axis=0, tiled=True)  26 us
    all_gather x1, waiting for transfers between devices, body(): lax.all_gather(query_matrix, 'sp', axis=0, tiled=True)  24.9 us
    all_gather x1, waiting for transfers between devices, body(): lax.all_gather(value_weight, 'sp', axis=0, tiled=True)  24.8 us
    all_gather x1, waiting for transfers between devices, body(): gathered = lax.all_gather(normed, 'tp', axis=0, tiled=True)  23.6 us
    all_gather x1, waiting for transfers between devices, body(): lax.all_gather(gate_weight, 'sp', axis=0, tiled=True)  23.1 us
  transfers between devices with their start and end apart: 12, of which 10 were waited for; matrix products, arithmetic and copies ran while one was open for 15% of the time, Pallas kernels for 0%

commit v1 on v0

--- a/solution.py
+++ b/solution.py
@@ -9,6 +9,11 @@
 EPSILON = 1e-06
 ROTARY_BASE = 10000.0
 HIGHEST_PRECISION = lax.Precision.HIGHEST
+
+
+def gathered_along(x, mesh_axis, d):
+    shards = lax.all_gather(x, mesh_axis)
+    return jnp.concatenate(shards, axis=d)
 
 
 def prefix_2(x, axis, join, neutral):
@@ -165,7 +170,7 @@
     ).astype(jnp.bfloat16)
     conv_rows_weight, ret_rows_weight = (
         lax.all_gather(conv_out_weight, "sp", axis=1, tiled=True),
-        lax.all_gather(ret_out_weight, "sp", axis=1, tiled=True),
+        gathered_along(ret_out_weight, "sp", 1),
     )
     return lax.psum_scatter(
         (

time: 345 us -> 345 us (level)
    all_gather x1, waiting for transfers between devices: 28.8 us -> 0.74 us  [gathered_along(): shards = lax.all_gather(x, mesh_axis)]
    all_gather x1, waiting for transfers between devices: 0.74 us -> 26.6 us  [body(): lax.all_gather(key_weight, 'sp', axis=0, tiled=True)]
  transfers between devices with their start and end apart: 12 -> 12, of which waited for: 10 -> 11; matrix products, arithmetic and copies ran while one was open for 15% -> 16% of each run, Pallas kernels for 0% -> 0%
where the time goes in v1:
time: 345 us
  waiting for transfers between devices  232 us (67%)
  blocking collectives  31.1 us (9%)
  matrix products  29.1 us (8%)
  local copies, waits for them, and re-layouts  17.8 us (5%)
  other arithmetic  15.9 us (5%)
  between operations  14.2 us (4%)
  starting transfers between devices  4.32 us (1%)
    reduce_scatter x1, waiting for transfers between devices, body(): lax.psum_scatter((jnp.dot(conv_branch, conv_rows_weight, preferred_elemen...  30.7 us
    all_gather x1, waiting for transfers between devices, body(): lax.all_gather(conv_out_weight, 'sp', axis=1, tiled=True)  29 us
    all_gather x1, waiting for transfers between devices, body(): lax.all_gather(key_weight, 'sp', axis=0, tiled=True)  26.6 us
    all_gather x1, waiting for transfers between devices, body(): lax.all_gather(conv_inner_weight, 'sp', axis=0, tiled=True)  26.1 us
    all_gather x1, waiting for transfers between devices, body(): lax.all_gather(value_weight, 'sp', axis=0, tiled=True)  24.8 us
    all_gather x1, waiting for transfers between devices, body(): lax.all_gather(query_matrix, 'sp', axis=0, tiled=True)  24.8 us
    all_gather x1, waiting for transfers between devices, body(): gathered = lax.all_gather(normed, 'tp', axis=0, tiled=True)  23.5 us
    all_gather x1, waiting for transfers between devices, body(): lax.all_gather(gate_weight, 'sp', axis=0, tiled=True)  22.3 us
  transfers between devices with their start and end apart: 12, of which 11 were waited for; matrix products, arithmetic and copies ran while one was open for 16% of the time, Pallas kernels for 0%

profile of v1, /device:TPU:0, one launch (start us, length us, event | category | flops | bytes accessed | tf_op | source)
XLA Modules:
  0.0 344.6 jit_solution(9947263242871581523)
XLA Ops:
  6.5 0.7 all-gather.32.cloned.1.call-update
  7.3 0.7 all-gather.26.cloned.1.call-update
  8.1 0.7 convert_element_type.96
  8.8 1.2 fusion.9
  10.0 2.0 fusion.11
  13.9 0.7 all-gather.18.cloned.1.call-update
  14.6 0.7 all-gather.16.cloned.1.call-update
  15.4 0.7 all-gather.22.cloned.1.call-update
  20.9 14.0 %all-reduce = bf16[8]{0:T(256)(128)(2,1)S(1)} all-reduce(bf16[8]{0:T(256)(128)(2,1)S(1)} %dynamic-update-slice), channel_id=2, replica_groups=mesh['grp'=2,'sp'=4,'tp'=4] {'sp'}, use_global_device_ids=true, to_apply=%add | all-reduce | flops 8 | bytes 32
  34.9 0.7 reshape.184
  37.4 1.8 multiply_cosine_fusion
  39.2 0.7 all-gather.32.cloned.1.call-done
  39.9 2.3 copy.112
  42.3 26.6 %all-gather.26.cloned.1.call-done = bf16[2048,256]{1,0:T(8,128)(2,1)} async-done(((bf16[512,256]{1,0:T(8,128)(2,1)}), bf16[2048,256]{1,0:T(8,128)(2,1)}) %all-gather.26.cloned.1.call-update) | async-done | bytes 1048592 | tf_op jit(solution)/shard_map/all_gather | solution.py:98
  68.9 23.5 %all-gather.14.cloned.1.call-done = bf16[512,2048]{1,0:T(8,128)(2,1)} async-done(((bf16[128,2048]{1,0:T(8,128)(2,1)}), bf16[512,2048]{1,0:T(8,128)(2,1)}) %all-gather.14.cloned.1.call-update) | async-done | bytes 2097168 | tf_op jit(solution)/shard_map/all_gather | solution.py:91
  92.4 2.6 convolution_convert_fusion.2
  95.1 1.0 copy.121
  96.1 1.0 copy.122
  97.1 24.8 %all-gather.28.cloned.1.call-done = bf16[2048,256]{1,0:T(8,128)(2,1)} async-done(((bf16[512,256]{1,0:T(8,128)(2,1)}), bf16[2048,256]{1,0:T(8,128)(2,1)}) %all-gather.28.cloned.1.call-update) | async-done | bytes 1048592 | tf_op jit(solution)/shard_map/all_gather | solution.py:97
  121.8 2.0 convolution_convert_fusion.1
  123.9 1.0 copy.123
  124.9 1.0 copy.124
  125.9 24.8 %all-gather.24.cloned.1.call-done = bf16[2048,256]{1,0:T(8,128)(2,1)} async-done(((bf16[512,256]{1,0:T(8,128)(2,1)}), bf16[2048,256]{1,0:T(8,128)(2,1)}) %all-gather.24.cloned.1.call-update) | async-done | bytes 1048592 | tf_op jit(solution)/shard_map/all_gather | solution.py:99
  150.6 1.9 convolution_convert_fusion.3
  152.7 2.9 multiply_subtract_fusion
  155.5 1.7 fusion.23
  157.2 9.3 %while.26 = (s32[]{:T(128)}, f32[2,128,128]{2,1,0:T(8,128)S(1)}, f32[4,2,128,128]{3,2,1,0:T(8,128)}, f32[4,2]{1,0:T(4,128)}, f32[4,2,128,128]{3,2,1,0:T(8,128)}, /*index=5*/s32[]{:T(128)}, s32[]{:T(128)}) while((s32[]{:T(128)}, f32[2,128,128]{2,1,0:T(8,128)S(1)}, f32[4,2,128,128]{3,2,1,0:T(8,128)}, f32[4,2]{1,0:T(4,128)}, ...), condition=%wide.region_2.3_spmd.clone, body=%wide.region_1.2_spmd.clone.sunk | while | flops 131075 | bytes 655992 | solution.py:145
  158.5 1.0 bitcast_add_fusion.2
  159.5 0.7 bitcast_dynamic-update-slice_fusion.2
  160.9 1.0 bitcast_add_fusion.2
  161.9 0.7 bitcast_dynamic-update-slice_fusion.2
  163.2 1.0 bitcast_add_fusion.2
  165.5 1.0 bitcast_add_fusion.2
  166.5 17.1 %all-gather.1 = bf16[8,128,128]{2,1,0:T(8,128)(2,1)} all-gather(bf16[2,128,128]{2,1,0:T(8,128)(2,1)S(1)} %convert_element_type.112), channel_id=3, replica_groups=mesh['grp'=2,'sp'=4,'tp'=4] {'sp'}, dimensions={0}, use_global_device_ids=true | all-gather | bytes 327680 | tf_op jit(solution)/shard_map/all_gather | solution.py:22
  183.8 2.7 fusion.7
  186.5 26.1 %all-gather.18.cloned.1.call-done = bf16[2048,256]{1,0:T(8,128)(2,1)} async-done(((bf16[512,256]{1,0:T(8,128)(2,1)}), bf16[2048,256]{1,0:T(8,128)(2,1)}) %all-gather.18.cloned.1.call-update) | async-done | bytes 1048592 | tf_op jit(solution)/shard_map/all_gather | solution.py:95
  212.6 2.2 fusion.6
  215.4 3.9 %collective-permute-start = (f32[2,256]{1,0:T(2,128)}, f32[2,256]{1,0:T(2,128)}, u32[]{:S(2)}, u32[]{:S(2)}) collective-permute-start(f32[2,256]{1,0:T(2,128)} %slice.45), channel_id=1, source_target_pairs={{0,4},{4,8},{8,12},{1,5},{5,9},{9,13},{2,6},{6,10},{10,14},{3,7},{... | collective-permute-start | bytes 6152 | tf_op jit(solution)/shard_map/ppermute | solution.py:42
  219.6 1.3 fusion.3
  221.4 1.1 multiply_reduce_fusion
  222.7 1.1 copy.110
  223.8 17.8 %all-gather.16.cloned.1.call-done = bf16[2048,256]{1,0:T(8,128)(2,1)} async-done(((bf16[512,256]{1,0:T(8,128)(2,1)}), bf16[2048,256]{1,0:T(8,128)(2,1)}) %all-gather.16.cloned.1.call-update) | async-done | bytes 1048592 | tf_op jit(solution)/shard_map/all_gather | solution.py:94
  241.6 29.0 %all-gather.22.cloned.1.call-done = bf16[256,2048]{1,0:T(8,128)(2,1)} async-done(((bf16[256,512]{1,0:T(8,128)(2,1)}), bf16[256,2048]{1,0:T(8,128)(2,1)}) %all-gather.22.cloned.1.call-update) | async-done | bytes 1048592 | tf_op jit(solution)/shard_map/all_gather | solution.py:172
  270.6 6.5 %fusion.30 = f32[512,2048]{1,0:T(8,128)} fusion(bf16[256,2048]{1,0:T(8,128)(2,1)} %all-gather.22.cloned.1.call-done, f32[2,256]{1,0:T(2,128)} %collective-permute-done, f32[512,256]{1,0:T(8,128)} %copy-done.2, bf16[512,2048]{1,0:T(8,128)(2,1)S(1)} %copy-done, bf16[2048,256]{1,0:T(8,128)(2,1)} %all-gather.16.cloned.1.call-done, f32[256]{0:T(256)S(1)} %bitcast.107, ...), kind=kOutput, calls=%fused_computation.62 | convolution fusion | flops 1075183616 | bytes 8918016 | tf_op jit(solution)/shard_map/dot_general | solution.py:177
  277.1 22.3 %all-gather.30.cloned.1.call-done = bf16[2048,256]{1,0:T(8,128)(2,1)} async-done(((bf16[512,256]{1,0:T(8,128)(2,1)}), bf16[2048,256]{1,0:T(8,128)(2,1)}) %all-gather.30.cloned.1.call-update) | async-done | bytes 1048592 | tf_op jit(solution)/shard_map/all_gather | solution.py:100
  299.4 1.4 mul.252
  300.8 6.5 %add_convert_fusion = bf16[512,2048]{1,0:T(8,128)(2,1)} fusion(f32[512,2048]{1,0:T(8,128)} %fusion.30, bf16[256,2048]{0,1:T(8,128)(2,1)S(1)} %bitcast.98, f32[64,8,2,128]{3,2,1,0:T(2,128)} %bitcast.100, f32[64,8,2,128]{3,2,1,0:T(2,128)} %bitcast.99, bf16[512,2048]{1,0:T(8,128)(2,1)S(1)} %copy-done, bf16[2048,256]{1,0:T(8,128)(2,1)} %all-gather.30.cloned.1.call-done), kind=kOutput, calls=%fused_computation.6 | convolution fusion | flops 1077018624 | bytes 11534336 | tf_op jit(solution)/shard_map/dot_general | solution.py:178
  307.3 30.7 %reduce-scatter.2.cloned.1.call-done = bf16[128,2048]{1,0:T(8,128)(2,1)} async-done(((bf16[512,2048]{1,0:T(8,128)(2,1)}), bf16[128,2048]{1,0:T(8,128)(2,1)}) %reduce-scatter.2.cloned.1.call-update) | async-done | bytes 524304 | tf_op jit(solution)/shard_map/reduce_scatter | solution.py:175
  (91 shorter events, 13.7 us)
Async XLA Ops:
  6.5 33.4 %all-gather.32.cloned.1.call-start = ((), (), s32[]{:S(2)}) async-start(), calls=%async_computation.11 | async-start | bytes 1310720 | tf_op jit(solution)/shard_map/all_gather | solution.py:15
  7.3 9.5 %copy-start.14 = (f32[512,2]{0,1:T(2,128)S(1)}, f32[512,2]{0,1:T(2,128)}, u32[]{:S(2)}) copy-start(f32[512,2]{0,1:T(2,128)} %param.29) | copy-start | bytes 12292
  7.3 61.6 %all-gather.26.cloned.1.call-start = ((), (), s32[]{:S(2)}) async-start(), calls=%async_computation.7 | async-start | bytes 1310720 | tf_op jit(solution)/shard_map/all_gather | solution.py:98
  8.0 10.7 %copy-start.15 = (u32[32]{0:T(128)S(1)}, u32[32]{0:T(128)}, u32[]{:S(2)}) copy-start(u32[32]{0:T(128)} %constant.65) | copy-start | bytes 388
  8.0 28.8 %copy-start.10 = (bf16[3,256]{1,0:T(4,128)(2,1)S(1)}, bf16[3,256]{1,0:T(4,128)(2,1)}, u32[]{:S(2)}) copy-start(bf16[3,256]{1,0:T(4,128)(2,1)} %param.26) | copy-start | bytes 4612
  8.0 84.4 %all-gather.14.cloned.1.call-start = ((), (), s32[]{:S(2)}) async-start(), calls=%async_computation.1 | async-start | bytes 2621440 | tf_op jit(solution)/shard_map/all_gather | solution.py:91
  12.1 109.8 %all-gather.28.cloned.1.call-start = ((), (), s32[]{:S(2)}) async-start(), calls=%async_computation.8 | async-start | bytes 1310720 | tf_op jit(solution)/shard_map/all_gather | solution.py:97
  12.6 138.0 %all-gather.24.cloned.1.call-start = ((), (), s32[]{:S(2)}) async-start(), calls=%async_computation.6 | async-start | bytes 1310720 | tf_op jit(solution)/shard_map/all_gather | solution.py:99
  13.2 170.5 %all-gather.20.cloned.1.call-start = ((), (), s32[]{:S(2)}) async-start(), calls=%async_computation.4 | async-start | bytes 1310720 | tf_op jit(solution)/shard_map/all_gather | solution.py:96
  13.8 198.8 %all-gather.18.cloned.1.call-start = ((), (), s32[]{:S(2)}) async-start(), calls=%async_computation.3 | async-start | bytes 1310720 | tf_op jit(solution)/shard_map/all_gather | solution.py:95
  14.6 227.0 %all-gather.16.cloned.1.call-start = ((), (), s32[]{:S(2)}) async-start(), calls=%async_computation.2 | async-start | bytes 1310720 | tf_op jit(solution)/shard_map/all_gather | solution.py:94
  15.3 255.3 %all-gather.22.cloned.1.call-start = ((), (), s32[]{:S(2)}) async-start(), calls=%async_computation.5 | async-start | bytes 1310720 | tf_op jit(solution)/shard_map/all_gather | solution.py:172
  16.0 283.3 %all-gather.30.cloned.1.call-start = ((), (), s32[]{:S(2)}) async-start(), calls=%async_computation.9 | async-start | bytes 1310720 | tf_op jit(solution)/shard_map/all_gather | solution.py:100
  16.6 321.4 %reduce-scatter.2.cloned.1.call-start = ((), (), s32[]{:S(2)}) async-start(), calls=%async_computation.10 | async-start | bytes 2621440 | tf_op jit(solution)/shard_map/reduce_scatter | solution.py:175
  95.0 26.8 %copy-start = (bf16[512,2048]{1,0:T(8,128)(2,1)S(1)}, bf16[512,2048]{1,0:T(8,128)(2,1)}, u32[]{:S(2)}) copy-start(bf16[512,2048]{1,0:T(8,128)(2,1)} %all-gather.14.cloned.1.call-done) | copy-start | bytes 6291460
  152.7 2.9 copy-start.8
  212.6 6.8 %copy-start.3 = (f32[512,2,64]{2,0,1:T(8,128)S(1)}, f32[512,2,64]{2,0,1:T(8,128)}, u32[]{:S(2)}) copy-start(f32[512,2,64]{2,0,1:T(8,128)} %get-tuple-element.145) | copy-start | bytes 786436
  212.6 6.8 %copy-start.4 = (f32[512,2,64]{2,0,1:T(8,128)S(1)}, f32[512,2,64]{2,0,1:T(8,128)}, u32[]{:S(2)}) copy-start(f32[512,2,64]{2,0,1:T(8,128)} %get-tuple-element.146) | copy-start | bytes 786436
  212.6 7.0 %copy-start.6 = (f32[4,128,2]{1,2,0:T(2,128)S(1)}, f32[4,128,2]{1,2,0:T(2,128)}, u32[]{:S(2)}) copy-start(f32[4,128,2]{1,2,0:T(2,128)} %copy.98) | copy-start | bytes 12292
  214.8 4.6 %copy-start.2 = (f32[512,256]{1,0:T(8,128)}, f32[512,256]{1,0:T(8,128)S(1)}, u32[]{:S(2)}) copy-start(f32[512,256]{1,0:T(8,128)S(1)} %fusion.6) | copy-start | bytes 1572868
  215.4 55.1 %collective-permute-start = (f32[2,256]{1,0:T(2,128)}, f32[2,256]{1,0:T(2,128)}, u32[]{:S(2)}, u32[]{:S(2)}) collective-permute-start(f32[2,256]{1,0:T(2,128)} %slice.45), channel_id=1, source_target_pairs={{0,4},{4,8},{8,12},{1,5},{5,9},{9,13},{2,6},{6,10},{10,14},{3,7},{... | collective-permute-start | bytes 6152 | tf_op jit(solution)/shard_map/ppermute | solution.py:42
  219.6 1.8 copy-start.5
  219.6 1.8 copy-start.7
  219.6 1.8 copy-start.9
  221.4 49.2 %copy-start.11 = (f32[1,256]{1,0:T(1,128)S(1)}, f32[1,256]{1,0:T(1,128)}, u32[]{:S(2)}) copy-start(f32[1,256]{1,0:T(1,128)} %get-tuple-element.159) | copy-start | bytes 3076
  221.4 49.2 %copy-start.12 = (f32[1,256]{1,0:T(1,128)S(1)}, f32[1,256]{1,0:T(1,128)}, u32[]{:S(2)}) copy-start(f32[1,256]{1,0:T(1,128)} %get-tuple-element.160) | copy-start | bytes 3076
  221.4 49.2 %copy-start.13 = (f32[1,256]{1,0:T(1,128)S(1)}, f32[1,256]{1,0:T(1,128)}, u32[]{:S(2)}) copy-start(f32[1,256]{1,0:T(1,128)} %get-tuple-element.161) | copy-start | bytes 3076
  270.6 30.2 %copy-start.1 = (bf16[256,4,512]{0,2,1:T(8,128)(2,1)S(1)}, bf16[256,4,512]{0,2,1:T(8,128)(2,1)}, u32[]{:S(2)}) copy-start(bf16[256,4,512]{0,2,1:T(8,128)(2,1)} %copy.112) | copy-start | bytes 3145732
Sparse Core Ops, SparseCore 0:
  8.9 30.9 all-gather.31
  41.5 27.3 all-gather.25
  70.4 21.9 all-gather.13
  93.8 27.9 all-gather.27
  123.3 27.3 all-gather.23
  152.1 31.6 all-gather.19
  185.3 27.2 all-gather.17
  214.2 27.3 all-gather.15
  243.2 27.3 all-gather.21
  272.0 27.3 all-gather.29
  307.5 30.5 reduce-scatter.1
